TPU v7x, 32 devices: a whole 2x2x4 slice. The times are simulated.
32 devices in a mesh: sp: 8 (over z, y), tp: 4 (over x, core).
Axes of the slice: x: 2, y: 2, z: 4, core: 2. Of those that a mesh axis runs over, the one named last changes fastest.
Arguments:
- queries: bfloat16 [5120, 1024], P('sp', 'tp'), may hold values from -6 to 6
- key_input: bfloat16 [5120, 1024], P('sp', 'tp'), may hold values from -6 to 6
- value_input: bfloat16 [5120, 1024], P('sp', 'tp'), may hold values from -6 to 6
- gate_input: bfloat16 [5120, 1024], P('sp', 'tp'), may hold values from -6 to 6
- log_decay: float32 [8, 5120], P('tp', 'sp'), may hold values from -1.6703125 to 0, as said below
- residual: bfloat16 [5120, 2048], P('sp'), may hold values from -52 to 52
- out_weight: bfloat16 [1024, 2048], P('tp'), may hold values from -0.375 to 0.375
- norm_gain: float32 [2048], replicated, may hold values from 0.3 to 2.7, as said below
- norm_bias: float32 [2048], replicated, may hold values from -1.8 to 1.8
- gate_weight: bfloat16 [2048, 5632], P('sp', 'tp'), may hold values from -0.125 to 0.125
- up_weight: bfloat16 [2048, 5632], P('sp', 'tp'), may hold values from -0.125 to 0.125
- down_weight: bfloat16 [5632, 2048], P('tp', 'sp'), may hold values from -0.078125 to 0.078125
- final_gain: float32 [2048], replicated, may hold values from 0.1 to 1.9
- final_bias: float32 [2048], replicated, may hold values from -1.8 to 1.8
Outputs:
- updated: bfloat16 [5120, 2048], P('sp', 'tp')
Inputs may be any that keep to these rules, and one draw needn't show every extreme that they name: `log_decay`: log-decays, never positive. `norm_gain`: positive gains.
All inputs are finite; a program needn't handle non-finite values.
Results may differ from a plain program's by a relative error of at most 0.023.
Values may be sent and summed in bfloat16 or wider, within the bound.
A program may use at most 128 MiB of HBM per device.

v0:
```python
import jax
import jax.numpy as jnp
from jax import lax
from jax.sharding import PartitionSpec as P

HD = 128
BLOCK = 128
ALPHA = 2.0**0.25
EPS = 1e-05
ROPE_BASE = 10000.0


def prefix(x, axis, combine, identity):
    peers, position = (lax.axis_size(axis), lax.axis_index(axis))
    everything = jax.tree.map(
        lambda part, kind: lax.all_gather(part.astype(kind), axis), x, (jnp.bfloat16, jnp.bfloat16)
    )
    start = jax.tree.map(
        lambda part, zero: jnp.broadcast_to(jnp.asarray(zero, part.dtype), part.shape), x, identity
    )

    def hop(k, before):
        reached = k < position
        new = combine(
            before, jax.tree.map(lambda part, own: part[k].astype(own.dtype), everything, x)
        )
        return jax.tree.map(lambda a, b: jnp.where(reached, a, b), new, before)

    return lax.fori_loop(0, peers, hop, start)


def rotate(values, positions):
    half = values.shape[-1] // 2
    freqs = ROPE_BASE ** (-2.0 * jnp.arange(half, dtype=jnp.float32) / values.shape[-1])
    angles = positions[:, None] * freqs[None, :]
    cosine = jnp.cos(angles)[:, None, :]
    sine = jnp.sin(angles)[:, None, :]
    first = values[..., :half]
    latter_operand = values[..., half:]
    return jnp.concatenate(
        [first * cosine - latter_operand * sine, first * sine + latter_operand * cosine], axis=-1
    )


def head_norm(retained):
    center = retained - jnp.mean(retained, axis=-1, keepdims=True)
    spread = jnp.mean(center * center, axis=-1, keepdims=True)
    return center * lax.rsqrt(spread + EPS)


def combine_states(earlier, later):
    return (earlier[0] * later[0], later[1] + later[0][:, None, None] * earlier[1])


def shards(
    queries,
    key_input,
    value_input,
    gate_input,
    log_decay,
    residual,
    out_weight,
    norm_gain,
    norm_bias,
    gate_weight,
    up_weight,
    down_weight,
    final_gain,
    final_bias,
):
    rows = queries.shape[0]
    heads_here = queries.shape[1] // HD
    blocks = rows // BLOCK
    offset = lax.axis_index("sp") * rows
    positions = (offset + jnp.arange(rows, dtype=jnp.int32)).astype(jnp.float32)
    shaped = (rows, heads_here, HD)
    per_block = (blocks, BLOCK, heads_here, HD)
    turned_q = (
        rotate(queries.astype(jnp.float32).reshape(shaped), positions)
        .astype(jnp.bfloat16)
        .reshape(per_block)
    )
    turned_k = (
        rotate(key_input.astype(jnp.float32).reshape(shaped), positions)
        .astype(jnp.bfloat16)
        .reshape(per_block)
    )
    value_blocks = value_input.reshape(per_block)
    cumul = jnp.cumsum(
        jnp.transpose(log_decay.reshape(heads_here, blocks, BLOCK), (1, 0, 2)), axis=2
    )
    cumul_rows = jnp.transpose(cumul, (0, 2, 1))
    lower = jnp.arange(BLOCK)[:, None] >= jnp.arange(BLOCK)[None, :]
    gaps = cumul[:, :, :, None] - cumul[:, :, None, :]
    damping = jnp.where(lower[None, None], jnp.exp(jnp.minimum(gaps, 0.0)), 0.0)
    scores = jnp.einsum("nihd,njhd->nhij", turned_q, turned_k, preferred_element_type=jnp.float32)
    weights = (scores * damping).astype(jnp.bfloat16)
    inner = jnp.einsum("nhij,njhe->nihe", weights, value_blocks, preferred_element_type=jnp.float32)
    ending = cumul[:, :, -1]
    value_broadened = value_blocks.astype(jnp.float32)
    keyed = turned_k.astype(jnp.float32) * jnp.exp(ending[:, None, :] - cumul_rows)[:, :, :, None]
    fresh = jnp.einsum("njhd,njhe->nhde", keyed, value_broadened, precision=lax.Precision.HIGHEST)

    def advance(state, pieces):
        decay_here, fresh_here = pieces
        return (jnp.exp(decay_here)[:, None, None] * state + fresh_here, state)

    local_state, prefixes = lax.scan(
        advance, jnp.zeros((heads_here, HD, HD), jnp.float32), (ending, fresh)
    )
    before = jnp.cumsum(ending, axis=0) - ending
    device_decay = jnp.exp(jnp.sum(ending, axis=0))
    scanned = prefix(
        (device_decay, local_state),
        "sp",
        combine_states,
        (jnp.ones_like(device_decay), jnp.zeros_like(local_state)),
    )
    entering = prefixes + jnp.exp(before)[:, :, None, None] * scanned[1][None]
    query_wide = turned_q.astype(jnp.float32) * jnp.exp(cumul_rows)[:, :, :, None]
    outer = jnp.einsum("nihd,nhde->nihe", query_wide, entering, precision=lax.Precision.HIGHEST)
    normed = head_norm((inner + outer).reshape(shaped)).reshape(rows, heads_here * HD)
    mixed_heads = (jax.nn.silu(gate_input.astype(jnp.float32)) * normed).astype(jnp.bfloat16)
    partial_value = jnp.dot(mixed_heads, out_weight, preferred_element_type=jnp.float32)
    width = residual.shape[1]
    col_width = width // lax.axis_size("tp")
    col_start = lax.axis_index("tp") * col_width

    def own_columns(array):
        return lax.dynamic_slice_in_dim(array, col_start, col_width, array.ndim - 1)

    mix = lax.psum(partial_value.astype(jnp.bfloat16), "tp")
    leading_sum = ALPHA * residual.astype(jnp.float32) + mix.astype(jnp.float32)
    center = leading_sum - jnp.mean(leading_sum, axis=1, keepdims=True)
    spread = jnp.mean(center * center, axis=1, keepdims=True)
    settled = (center * lax.rsqrt(spread + EPS) * norm_gain + norm_bias).astype(jnp.bfloat16)
    settled_cols = own_columns(settled)

    def add_rows(piece):
        return jnp.dot(settled, piece, preferred_element_type=jnp.float32)

    gate_acts = add_rows(lax.all_gather(gate_weight, "sp", axis=0, tiled=True))
    lifted = add_rows(lax.all_gather(up_weight, "sp", axis=0, tiled=True))
    latent_width = (jax.nn.silu(gate_acts) * lifted).astype(jnp.bfloat16)
    terms = jnp.dot(
        latent_width,
        lax.all_gather(down_weight, "sp", axis=1, tiled=True),
        preferred_element_type=jnp.float32,
    )
    ffn_cols = lax.psum_scatter(terms.astype(jnp.bfloat16), "tp", scatter_dimension=1, tiled=True)
    second_sum = ALPHA * settled_cols.astype(jnp.float32) + ffn_cols.astype(jnp.float32)
    totals_two, squares_two = lax.psum(
        (jnp.sum(second_sum, axis=1), jnp.sum(second_sum * second_sum, axis=1)), "tp"
    )
    average_two = totals_two / width
    spread_two = squares_two / width - average_two * average_two
    scaled_two = (second_sum - average_two[:, None]) * lax.rsqrt(spread_two + EPS)[:, None]
    return (scaled_two * own_columns(final_gain) + own_columns(final_bias)).astype(jnp.bfloat16)


def solution(mesh):
    in_specs = (
        P("sp", "tp"),
        P("sp", "tp"),
        P("sp", "tp"),
        P("sp", "tp"),
        P("tp", "sp"),
        P("sp", None),
        P("tp", None),
        P(),
        P(),
        P("sp", "tp"),
        P("sp", "tp"),
        P("tp", "sp"),
        P(),
        P(),
    )
    out_specs = P("sp", "tp")
    return jax.shard_map(shards, mesh=mesh, in_specs=in_specs, out_specs=out_specs, check_vma=False)
```

profile of v0, /device:TPU:0, one launch (start us, length us, event | category | flops | bytes accessed | tf_op | source)
XLA Modules:
  0.0 434.6 jit_solution(10507391402819925788)
XLA Ops:
  7.5 1.2 copy.65
  8.7 1.1 copy.66
  9.9 0.6 multiply_cosine_fusion
  10.5 0.9 subtract_convert_fusion.1
  11.6 0.3 copy.49
  12.1 0.3 copy.50
  12.4 1.5 reduce_window_sum.22
  14.5 1.0 fusion.16
  15.5 3.9 while.29
  15.5 0.7 bitcast_dynamic-update-slice_fusion.3
  16.3 0.7 bitcast_dynamic-update-slice_fusion.3
  17.1 0.7 bitcast_dynamic-update-slice_fusion.3
  17.9 0.7 bitcast_dynamic-update-slice_fusion.3
  18.6 0.7 bitcast_dynamic-update-slice_fusion.3
  19.4 33.0 %all-gather = bf16[16,128,128]{2,1,0:T(8,128)(2,1)S(1)} all-gather(bf16[2,128,128]{2,1,0:T(8,128)(2,1)S(1)} %convert_element_type.101), channel_id=2, replica_groups=mesh['sp'=8,'tp'=4] {'sp'}, dimensions={0}, use_global_device_ids=true | all-gather | bytes 589824 | tf_op jit(solution)/shard_map/all_gather | solution.py:16
  52.5 0.6 dynamic-slice
  53.7 0.2 dynamic-update-slice
  54.2 21.5 %all-reduce = bf16[16]{0:T(256)(128)(2,1)S(1)} all-reduce(bf16[16]{0:T(256)(128)(2,1)S(1)} %dynamic-update-slice), channel_id=3, replica_groups=mesh['sp'=8,'tp'=4] {'sp'}, use_global_device_ids=true, to_apply=%add | all-reduce | flops 16 | bytes 64
  75.8 1.0 while.30
  76.8 1.1 concatenate.18
  77.9 0.3 copy.45
  78.2 1.1 concatenate.19
  79.3 0.3 copy.46
  79.7 3.5 convolution_bitcast_fusion
  83.1 1.9 fusion.44
  85.1 0.9 copy.60
  86.5 0.8 mul.258
  87.3 0.8 sub.78
  88.2 2.5 convolution_convert_fusion.1
  90.7 0.5 all-gather.6.cloned.1.call-update
  91.3 0.5 all-gather.10.cloned.1.call-update
  91.9 0.5 all-gather.8.cloned.1.call-update
  92.6 55.3 %all-reduce.4.cloned.1.call-done = bf16[640,2048]{1,0:T(8,128)(2,1)} async-done(((bf16[640,2048]{1,0:T(8,128)(2,1)}), bf16[640,2048]{1,0:T(8,128)(2,1)}) %all-reduce.4.cloned.1.call-update) | async-done | bytes 2621456 | tf_op jit(solution)/shard_map/psum | solution.py:132
  148.0 3.6 fusion.3
  151.7 0.5 copy-done.2
  152.1 1.3 multiply_reduce_fusion
  153.4 3.0 add_convert_fusion
  156.4 26.3 %all-gather.6.cloned.1.call-done = bf16[2048,1408]{1,0:T(8,128)(2,1)} async-done(((bf16[256,1408]{1,0:T(8,128)(2,1)}), bf16[2048,1408]{1,0:T(8,128)(2,1)}) %all-gather.6.cloned.1.call-update) | async-done | bytes 5767184 | tf_op jit(solution)/shard_map/all_gather | solution.py:142
  182.7 9.4 %fusion.45 = f32[640,1408]{1,0:T(8,128)} fusion(bf16[640,2048]{1,0:T(8,128)(2,1)} %add_convert_fusion, bf16[2048,1408]{1,0:T(8,128)(2,1)} %all-gather.6.cloned.1.call-done), kind=kOutput, calls=%fused_computation.87 | convolution fusion | flops 3690987520 | bytes 11993088 | tf_op jit(solution)/shard_map/dot_general | solution.py:140
  192.2 83.6 %all-gather.10.cloned.1.call-done = bf16[1408,2048]{1,0:T(8,128)(2,1)} async-done(((bf16[1408,256]{1,0:T(8,128)(2,1)}), bf16[1408,2048]{1,0:T(8,128)(2,1)}) %all-gather.10.cloned.1.call-update) | async-done | bytes 5767184 | tf_op jit(solution)/shard_map/all_gather | solution.py:147
  275.7 92.4 %all-gather.8.cloned.1.call-done = bf16[2048,1408]{1,0:T(8,128)(2,1)} async-done(((bf16[256,1408]{1,0:T(8,128)(2,1)}), bf16[2048,1408]{1,0:T(8,128)(2,1)}) %all-gather.8.cloned.1.call-update) | async-done | bytes 5767184 | tf_op jit(solution)/shard_map/all_gather | solution.py:143
  368.1 16.2 %convolution_convert_fusion = bf16[640,2048]{1,0:T(8,128)(2,1)} fusion(bf16[1408,2048]{1,0:T(8,128)(2,1)} %all-gather.10.cloned.1.call-done, bf16[640,2048]{1,0:T(8,128)(2,1)} %add_convert_fusion, bf16[2048,1408]{1,0:T(8,128)(2,1)} %all-gather.8.cloned.1.call-done, f32[640,1408]{1,0:T(8,128)} %fusion.45), kind=kOutput, calls=%fused_computation.14 | convolution fusion | flops 7388692480 | bytes 20381696 | tf_op jit(solution)/shard_map/dot_general | solution.py:145
  384.3 0.8 dynamic_slice.32
  385.1 0.8 dynamic_slice.33
  385.8 31.1 %reduce-scatter.2.cloned.1.call-done = bf16[640,512]{1,0:T(8,128)(2,1)} async-done(((bf16[640,2048]{1,0:T(8,128)(2,1)}), bf16[640,512]{1,0:T(8,128)(2,1)}) %reduce-scatter.2.cloned.1.call-update) | async-done | bytes 655376 | tf_op jit(solution)/shard_map/reduce_scatter | solution.py:150
  417.0 1.7 fusion.7
  418.6 5.9 %all-reduce.1 = (f32[640]{0:T(1024)S(1)}, f32[640]{0:T(1024)S(1)}) all-reduce(f32[640]{0:T(1024)S(1)} %get-tuple-element.182, f32[640]{0:T(1024)S(1)} %get-tuple-element.181), channel_id=1, replica_groups=mesh['sp'=8,'tp'=4] {'tp'}, use_global_device_ids=true, to_apply=%region_16.17 | all-reduce | flops 1280 | bytes 10240 | tf_op jit(solution)/shard_map/psum | solution.py:152
  424.5 2.5 add_convert_fusion.1
  (80 shorter events, 3.5 us)
Async XLA Ops:
  7.4 80.8 %copy-start = (bf16[256,2048]{1,0:T(8,128)(2,1)S(1)}, bf16[256,2048]{1,0:T(8,128)(2,1)}, u32[]{:S(2)}) copy-start(bf16[256,2048]{1,0:T(8,128)(2,1)} %param.24) | copy-start | bytes 3145732
  7.4 5.0 %copy-start.6 = (f32[2,640]{1,0:T(2,128)S(1)}, f32[2,640]{1,0:T(2,128)}, u32[]{:S(2)}) copy-start(f32[2,640]{1,0:T(2,128)} %param.22) | copy-start | bytes 15364
  7.4 7.0 %copy-start.3 = (bf16[640,256]{1,0:T(8,128)(2,1)S(1)}, bf16[640,256]{1,0:T(8,128)(2,1)}, u32[]{:S(2)}) copy-start(bf16[640,256]{1,0:T(8,128)(2,1)} %param.20) | copy-start | bytes 983044
  7.4 140.6 %all-reduce.4.cloned.1.call-start = ((), (), s32[]{:S(2)}) async-start(), calls=%async_computation.1 | async-start | bytes 5242880 | tf_op jit(solution)/shard_map/psum | solution.py:132
  12.1 40.4 %copy-start.8 = (u32[32]{0:T(128)S(1)}, u32[32]{0:T(128)}, u32[]{:S(2)}) copy-start(u32[32]{0:T(128)} %constant.93) | copy-start | bytes 388
  85.1 3.1 copy-start.7
  90.7 92.1 %all-gather.6.cloned.1.call-start = ((), (), s32[]{:S(2)}) async-start(), calls=%async_computation.2 | async-start | bytes 6488064 | tf_op jit(solution)/shard_map/all_gather | solution.py:142
  91.2 184.5 %all-gather.10.cloned.1.call-start = ((), (), s32[]{:S(2)}) async-start(), calls=%async_computation.4 | async-start | bytes 6488064 | tf_op jit(solution)/shard_map/all_gather | solution.py:147
  91.8 276.3 %all-gather.8.cloned.1.call-start = ((), (), s32[]{:S(2)}) async-start(), calls=%async_computation.3 | async-start | bytes 6488064 | tf_op jit(solution)/shard_map/all_gather | solution.py:143
  92.4 324.6 %reduce-scatter.2.cloned.1.call-start = ((), (), s32[]{:S(2)}) async-start(), calls=%async_computation.5 | async-start | bytes 3276800 | tf_op jit(solution)/shard_map/reduce_scatter | solution.py:150
  148.0 3.7 copy-start.1
  148.0 4.2 copy-start.2
  151.6 1.8 copy-start.4
  151.6 1.8 copy-start.5
Sparse Core Ops, SparseCore 0:
  90.8 57.1 all-reduce.3
  384.4 32.4 reduce-scatter.1
Sparse Core Ops, SparseCore 1:
  93.3 89.3 all-gather.5
  184.7 91.0 all-gather.9
  277.8 90.3 all-gather.7
where the time goes:
time: 435 us
  waiting for transfers between devices  290 us (67%)
  blocking collectives  60.4 us (14%)
  matrix products  34.4 us (8%)
  other arithmetic  20.3 us (5%)
  between operations  16 us (4%)
  local copies, waits for them, and re-layouts  12.4 us (3%)
    all_gather x1, waiting for transfers between devices, shards(): lifted = add_rows(lax.all_gather(up_weight, 'sp', axis=0, tiled=True))  92.4 us
    all_gather x1, waiting for transfers between devices, shards(): lax.all_gather(down_weight, 'sp', axis=1, tiled=True)  83.6 us
    psum x1, waiting for transfers between devices, shards(): mix = lax.psum(partial_value.astype(jnp.bfloat16), 'tp')  55.3 us
    all_gather x1, blocking collectives, prefix(): lax.all_gather(part.astype(kind), axis)  33 us
    reduce_scatter x1, waiting for transfers between devices, shards(): lax.psum_scatter(terms.astype(jnp.bfloat16), 'tp', scatter_dimension=1, t...  31.1 us
    all_gather x1, waiting for transfers between devices, shards(): gate_acts = add_rows(lax.all_gather(gate_weight, 'sp', axis=0, tiled=True))  26.3 us
    unnamed x1, blocking collectives  21.5 us
    dot_general x1, matrix products, shards(): jnp.dot(latent_width, lax.all_gather(down_weight, 'sp', axis=1, tiled=Tru...  16.2 us
  transfers between devices with their start and end apart: 5, of which 5 were waited for; matrix products, arithmetic and copies ran while one was open for 4% of the time, Pallas kernels for 0%

commit v1 on v0

--- a/solution.py
+++ b/solution.py
@@ -8,6 +8,12 @@
 ALPHA = 2.0**0.25
 EPS = 1e-05
 ROPE_BASE = 10000.0
+
+
+def fix_the_weights(vec):
+    raw_out = jax.lax.all_gather(vec, "tp")
+    b_now = jnp.sum(raw_out, 0)
+    return b_now
 
 
 def prefix(x, axis, combine, identity):
@@ -129,7 +135,7 @@
     def own_columns(array):
         return lax.dynamic_slice_in_dim(array, col_start, col_width, array.ndim - 1)
 
-    mix = lax.psum(partial_value.astype(jnp.bfloat16), "tp")
+    mix = fix_the_weights(partial_value.astype(jnp.bfloat16))
     leading_sum = ALPHA * residual.astype(jnp.float32) + mix.astype(jnp.float32)
     center = leading_sum - jnp.mean(leading_sum, axis=1, keepdims=True)
     spread = jnp.mean(center * center, axis=1, keepdims=True)

time: 435 us -> 504 us (1.16)
  waiting for transfers between devices: 290 us -> 352 us
  other arithmetic: 20.3 us -> 29.4 us
    all_gather x0 -> x1, waiting for transfers between devices: none -> 65.3 us  [fix_the_weights(): raw_out = jax.lax.all_gather(vec, 'tp')]
    psum x1 -> x0, waiting for transfers between devices: 55.3 us -> none  [shards(): mix = lax.psum(partial_value.astype(jnp.bfloat16), 'tp')]
    all_gather x1, waiting for transfers between devices: 26.3 us -> 76.7 us  [shards(): gate_acts = add_rows(lax.all_gather(gate_weight, 'sp', axis=0, tiled=True))]
    all_gather x1, waiting for transfers between devices: 83.6 us -> 93.2 us  [shards(): lax.all_gather(down_weight, 'sp', axis=1, tiled=True)]
    all_gather x1, waiting for transfers between devices: 92.4 us -> 83.3 us  [shards(): lifted = add_rows(lax.all_gather(up_weight, 'sp', axis=0, tiled=True))]
    reduce_sum x0 -> x1, other arithmetic: none -> 8.83 us  [fix_the_weights(): b_now = jnp.sum(raw_out, 0)]
  transfers between devices with their start and end apart: 5 -> 5, of which waited for: 5 -> 5; matrix products, arithmetic and copies ran while one was open for 4% -> 6% of each run, Pallas kernels for 0% -> 0%
where the time goes in v1:
time: 504 us
  waiting for transfers between devices  352 us (70%)
  blocking collectives  60.4 us (12%)
  matrix products  34.7 us (7%)
  other arithmetic  29.4 us (6%)
  between operations  14.1 us (3%)
  local copies, waits for them, and re-layouts  12.6 us (2%)
    all_gather x1, waiting for transfers between devices, shards(): lax.all_gather(down_weight, 'sp', axis=1, tiled=True)  93.2 us
    all_gather x1, waiting for transfers between devices, shards(): lifted = add_rows(lax.all_gather(up_weight, 'sp', axis=0, tiled=True))  83.3 us
    all_gather x1, waiting for transfers between devices, shards(): gate_acts = add_rows(lax.all_gather(gate_weight, 'sp', axis=0, tiled=True))  76.7 us
    all_gather x1, waiting for transfers between devices, fix_the_weights(): raw_out = jax.lax.all_gather(vec, 'tp')  65.3 us
    all_gather x1, blocking collectives, prefix(): lax.all_gather(part.astype(kind), axis)  33 us
    reduce_scatter x1, waiting for transfers between devices, shards(): lax.psum_scatter(terms.astype(jnp.bfloat16), 'tp', scatter_dimension=1, t...  31.2 us
    unnamed x1, blocking collectives  21.5 us
    dot_general x1, matrix products, shards(): jnp.dot(latent_width, lax.all_gather(down_weight, 'sp', axis=1, tiled=Tru...  16.4 us
  transfers between devices with their start and end apart: 5, of which 5 were waited for; matrix products, arithmetic and copies ran while one was open for 6% of the time, Pallas kernels for 0%

profile of v1, /device:TPU:0, one launch (start us, length us, event | category | flops | bytes accessed | tf_op | source)
XLA Modules:
  0.0 503.6 jit_solution(12840674363275344268)
XLA Ops:
  6.6 1.2 copy.65
  7.9 1.1 copy.66
  9.0 0.6 multiply_cosine_fusion
  9.7 0.9 subtract_convert_fusion.1
  10.8 0.3 copy.49
  11.2 0.3 copy.50
  11.6 1.5 reduce_window_sum.22
  13.7 1.0 fusion.16
  14.6 3.9 while.29
  14.7 0.7 bitcast_dynamic-update-slice_fusion.3
  15.4 0.7 bitcast_dynamic-update-slice_fusion.3
  16.2 0.7 bitcast_dynamic-update-slice_fusion.3
  17.0 0.7 bitcast_dynamic-update-slice_fusion.3
  17.8 0.7 bitcast_dynamic-update-slice_fusion.3
  18.6 33.0 %all-gather = bf16[16,128,128]{2,1,0:T(8,128)(2,1)S(1)} all-gather(bf16[2,128,128]{2,1,0:T(8,128)(2,1)S(1)} %convert_element_type.103), channel_id=2, replica_groups=mesh['sp'=8,'tp'=4] {'sp'}, dimensions={0}, use_global_device_ids=true | all-gather | bytes 589824 | tf_op jit(solution)/shard_map/all_gather | solution.py:22
  51.7 0.6 dynamic-slice
  53.3 21.5 %all-reduce = bf16[16]{0:T(256)(128)(2,1)S(1)} all-reduce(bf16[16]{0:T(256)(128)(2,1)S(1)} %dynamic-update-slice), channel_id=3, replica_groups=mesh['sp'=8,'tp'=4] {'sp'}, use_global_device_ids=true, to_apply=%add | all-reduce | flops 16 | bytes 64
  74.9 1.0 while.30
  75.9 1.1 concatenate.18
  77.1 0.3 copy.45
  77.3 1.1 concatenate.19
  78.5 0.3 copy.46
  78.8 3.5 convolution_bitcast_fusion
  82.3 1.9 fusion.44
  84.2 0.9 copy.60
  85.6 0.8 mul.258
  86.5 0.8 sub.78
  87.3 2.6 convolution_convert_fusion.1
  89.9 0.7 all-gather.8.cloned.1.call-update
  90.7 0.7 all-gather.10.cloned.1.call-update
  91.4 0.5 all-gather.12.cloned.1.call-update
  92.2 65.3 %all-gather.14.cloned.1.call-done = bf16[2560,2048]{1,0:T(8,128)(2,1)} async-done(((bf16[640,2048]{1,0:T(8,128)(2,1)}), bf16[2560,2048]{1,0:T(8,128)(2,1)}) %all-gather.14.cloned.1.call-update) | async-done | bytes 10485776 | tf_op jit(solution)/shard_map/all_gather | solution.py:14
  157.5 8.8 %reduce_sum.78 = bf16[640,2048]{1,0:T(8,128)(2,1)} reduce(bf16[4,640,2048]{2,1,0:T(8,128)(2,1)} %bitcast.86, bf16[]{:T(256)} %constant.87.clone.1), dimensions={0}, to_apply=%region_9.10 | reduce | flops 3932160 | bytes 13107202 | tf_op jit(solution)/shard_map/reduce_sum | solution.py:15
  166.3 4.0 fusion.3
  170.3 0.7 copy-done.2
  171.0 1.3 multiply_reduce_fusion
  172.3 3.0 add_convert_fusion
  175.3 76.7 %all-gather.8.cloned.1.call-done = bf16[2048,1408]{1,0:T(8,128)(2,1)} async-done(((bf16[256,1408]{1,0:T(8,128)(2,1)}), bf16[2048,1408]{1,0:T(8,128)(2,1)}) %all-gather.8.cloned.1.call-update) | async-done | bytes 5767184 | tf_op jit(solution)/shard_map/all_gather | solution.py:148
  252.0 9.4 %fusion.45 = f32[640,1408]{1,0:T(8,128)} fusion(bf16[640,2048]{1,0:T(8,128)(2,1)} %add_convert_fusion, bf16[2048,1408]{1,0:T(8,128)(2,1)} %all-gather.8.cloned.1.call-done), kind=kOutput, calls=%fused_computation.87 | convolution fusion | flops 3690987520 | bytes 11993088 | tf_op jit(solution)/shard_map/dot_general | solution.py:146
  261.4 83.3 %all-gather.10.cloned.1.call-done = bf16[2048,1408]{1,0:T(8,128)(2,1)} async-done(((bf16[256,1408]{1,0:T(8,128)(2,1)}), bf16[2048,1408]{1,0:T(8,128)(2,1)}) %all-gather.10.cloned.1.call-update) | async-done | bytes 5767184 | tf_op jit(solution)/shard_map/all_gather | solution.py:149
  344.7 93.2 %all-gather.12.cloned.1.call-done = bf16[1408,2048]{1,0:T(8,128)(2,1)} async-done(((bf16[1408,256]{1,0:T(8,128)(2,1)}), bf16[1408,2048]{1,0:T(8,128)(2,1)}) %all-gather.12.cloned.1.call-update) | async-done | bytes 5767184 | tf_op jit(solution)/shard_map/all_gather | solution.py:153
  438.0 16.4 %convolution_convert_fusion = bf16[640,2048]{1,0:T(8,128)(2,1)} fusion(bf16[1408,2048]{1,0:T(8,128)(2,1)} %all-gather.12.cloned.1.call-done, bf16[640,2048]{1,0:T(8,128)(2,1)} %add_convert_fusion, bf16[2048,1408]{1,0:T(8,128)(2,1)} %all-gather.10.cloned.1.call-done, f32[640,1408]{1,0:T(8,128)} %fusion.45), kind=kOutput, calls=%fused_computation.14 | convolution fusion | flops 7388692480 | bytes 20381696 | tf_op jit(solution)/shard_map/dot_general | solution.py:151
  454.4 0.8 dynamic_slice.32
  455.1 0.8 dynamic_slice.33
  455.9 31.2 %reduce-scatter.2.cloned.1.call-done = bf16[640,512]{1,0:T(8,128)(2,1)} async-done(((bf16[640,2048]{1,0:T(8,128)(2,1)}), bf16[640,512]{1,0:T(8,128)(2,1)}) %reduce-scatter.2.cloned.1.call-update) | async-done | bytes 655376 | tf_op jit(solution)/shard_map/reduce_scatter | solution.py:156
  487.0 1.7 fusion.7
  488.7 5.9 %all-reduce.1 = (f32[640]{0:T(1024)S(1)}, f32[640]{0:T(1024)S(1)}) all-reduce(f32[640]{0:T(1024)S(1)} %get-tuple-element.182, f32[640]{0:T(1024)S(1)} %get-tuple-element.181), channel_id=1, replica_groups=mesh['sp'=8,'tp'=4] {'tp'}, use_global_device_ids=true, to_apply=%region_16.17 | all-reduce | flops 1280 | bytes 10240 | tf_op jit(solution)/shard_map/psum | solution.py:158
  494.6 2.5 add_convert_fusion.1
  (81 shorter events, 3.7 us)
Async XLA Ops:
  6.5 80.8 %copy-start = (bf16[256,2048]{1,0:T(8,128)(2,1)S(1)}, bf16[256,2048]{1,0:T(8,128)(2,1)}, u32[]{:S(2)}) copy-start(bf16[256,2048]{1,0:T(8,128)(2,1)} %param.24) | copy-start | bytes 3145732
  6.5 5.0 copy-start.6
  6.5 7.0 %copy-start.3 = (bf16[640,256]{1,0:T(8,128)(2,1)S(1)}, bf16[640,256]{1,0:T(8,128)(2,1)}, u32[]{:S(2)}) copy-start(bf16[640,256]{1,0:T(8,128)(2,1)} %param.20) | copy-start | bytes 983044
  6.5 150.9 %all-gather.14.cloned.1.call-start = ((), (), s32[]{:S(2)}) async-start(), calls=%async_computation.5 | async-start | bytes 13107200 | tf_op jit(solution)/shard_map/all_gather | solution.py:14
  11.2 40.4 %copy-start.8 = (u32[32]{0:T(128)S(1)}, u32[32]{0:T(128)}, u32[]{:S(2)}) copy-start(u32[32]{0:T(128)} %constant.95) | copy-start | bytes 388
  84.2 3.1 copy-start.7
  89.9 162.1 %all-gather.8.cloned.1.call-start = ((), (), s32[]{:S(2)}) async-start(), calls=%async_computation.1 | async-start | bytes 6488064 | tf_op jit(solution)/shard_map/all_gather | solution.py:148
  90.6 254.1 %all-gather.10.cloned.1.call-start = ((), (), s32[]{:S(2)}) async-start(), calls=%async_computation.2 | async-start | bytes 6488064 | tf_op jit(solution)/shard_map/all_gather | solution.py:149
  91.4 346.6 %all-gather.12.cloned.1.call-start = ((), (), s32[]{:S(2)}) async-start(), calls=%async_computation.3 | async-start | bytes 6488064 | tf_op jit(solution)/shard_map/all_gather | solution.py:153
  91.9 395.1 %reduce-scatter.2.cloned.1.call-start = ((), (), s32[]{:S(2)}) async-start(), calls=%async_computation.4 | async-start | bytes 3276800 | tf_op jit(solution)/shard_map/reduce_scatter | solution.py:156
  166.3 4.0 copy-start.1
  166.3 4.7 copy-start.2
  170.3 2.0 copy-start.4
  170.3 2.0 copy-start.5
Sparse Core Ops, SparseCore 0:
  90.0 67.4 all-gather.13
  159.6 92.3 all-gather.7
  254.2 90.4 all-gather.9
  346.6 91.2 all-gather.11
  454.5 32.5 reduce-scatter.1
